TPU v7x, 32 devices: a whole 2x2x4 slice. The times are simulated.
32 devices in a mesh: rep: 2 (over x), fs: 8 (over z, y), tp: 2 (over core).
Axes of the slice: x: 2, y: 2, z: 4, core: 2. Of those that a mesh axis runs over, the one named last changes fastest.
Arguments:
- later_input: bfloat16 [2048, 2048], P(('rep', 'fs')), may hold values from -6 to 6
- earlier_input: bfloat16 [2048, 2048], P(('rep', 'fs')), may hold values from -6 to 6
- cotangent: bfloat16 [2048, 2048], P(('rep', 'fs')), may hold values from -6 to 6
- gate_weight: bfloat16 [2048, 3072], P('fs', 'tp'), may hold values from -0.125 to 0.125
- up_weight: bfloat16 [2048, 3072], P('fs', 'tp'), may hold values from -0.125 to 0.125
- down_weight: bfloat16 [2048, 3072], P('fs', 'tp'), may hold values from -0.109375 to 0.109375
- gate_sum: float32 [2048, 3072], P('fs', 'tp'), may hold values from -192 to 192
- up_sum: float32 [2048, 3072], P('fs', 'tp'), may hold values from -192 to 192
- down_sum: float32 [2048, 3072], P('fs', 'tp'), may hold values from -192 to 192
Outputs:
- later_output: bfloat16 [2048, 2048], P(('rep', 'fs'))
- earlier_input_grad: bfloat16 [2048, 2048], P(('rep', 'fs'))
- gate_sum_new: float32 [2048, 3072], P('fs', 'tp')
- up_sum_new: float32 [2048, 3072], P('fs', 'tp')
- down_sum_new: float32 [2048, 3072], P('fs', 'tp')
All inputs are finite; a program needn't handle non-finite values.
Results may differ from a plain program's by a relative error of at most 0.02.
Values may be sent and summed in bfloat16 or wider, within the bound.
A program may use at most 128 MiB of HBM per device.

v0:
```python
import jax
import jax.numpy as jnp
from jax import lax
from jax.sharding import PartitionSpec as P


def contract_last(first, second):
    return lax.dot_general(
        first, second, (((1,), (1,)), ((), ())), preferred_element_type=jnp.float32
    )


def contract_first(first, second):
    return lax.dot_general(
        first, second, (((0,), (0,)), ((), ())), preferred_element_type=jnp.float32
    )


def per_device(
    later_input,
    earlier_input,
    cotangent,
    gate_weight,
    up_weight,
    down_weight,
    gate_sum,
    up_sum,
    down_sum,
):
    gate_full, up_full, down_full = (
        lax.all_gather(gate_weight, "fs", axis=0, tiled=True),
        lax.all_gather(up_weight, "fs", axis=0, tiled=True),
        lax.all_gather(down_weight, "fs", axis=0, tiled=True),
    )
    gate_late = jnp.dot(later_input, gate_full, preferred_element_type=jnp.float32)
    up_late = jnp.dot(later_input, up_full, preferred_element_type=jnp.float32)
    hidden_late = (jax.nn.silu(gate_late) * up_late).astype(jnp.bfloat16)
    partial_late = contract_last(hidden_late, down_full)
    later_output = lax.psum(partial_late.astype(jnp.bfloat16), "tp")
    gate_early = jnp.dot(earlier_input, gate_full, preferred_element_type=jnp.float32)
    up_early = jnp.dot(earlier_input, up_full, preferred_element_type=jnp.float32)
    hidden_grad = jnp.dot(cotangent, down_full, preferred_element_type=jnp.float32)
    sigmoid_gate = jax.nn.sigmoid(gate_early)
    silu_early = gate_early * sigmoid_gate
    gate_grad = (
        hidden_grad * up_early * sigmoid_gate * (1.0 + gate_early * (1.0 - sigmoid_gate))
    ).astype(jnp.bfloat16)
    up_grad = (hidden_grad * silu_early).astype(jnp.bfloat16)
    hidden_early = (silu_early * up_early).astype(jnp.bfloat16)
    partial_early = contract_last(gate_grad, gate_full) + contract_last(up_grad, up_full)
    earlier_input_grad = lax.psum(partial_early.astype(jnp.bfloat16), "tp")
    columns, cot_columns = (
        lax.all_to_all(earlier_input, "fs", split_axis=1, concat_axis=0, tiled=True),
        lax.all_to_all(cotangent, "fs", split_axis=1, concat_axis=0, tiled=True),
    )
    gate_local = contract_first(columns, lax.all_gather(gate_grad, "fs", axis=0, tiled=True))
    up_local = contract_first(columns, lax.all_gather(up_grad, "fs", axis=0, tiled=True))
    down_local = contract_first(cot_columns, lax.all_gather(hidden_early, "fs", axis=0, tiled=True))
    gate_total, up_total, down_total = (
        lax.psum(gate_local.astype(jnp.bfloat16), "rep").astype(jnp.float32),
        lax.psum(up_local.astype(jnp.bfloat16), "rep").astype(jnp.float32),
        lax.psum(down_local.astype(jnp.bfloat16), "rep").astype(jnp.float32),
    )
    return (
        later_output,
        earlier_input_grad,
        gate_sum + gate_total,
        up_sum + up_total,
        down_sum + down_total,
    )


def solution(mesh):
    placed = (
        P(("rep", "fs"), None),
        P(("rep", "fs"), None),
        P(("rep", "fs"), None),
        P("fs", "tp"),
        P("fs", "tp"),
        P("fs", "tp"),
        P("fs", "tp"),
        P("fs", "tp"),
        P("fs", "tp"),
    )
    return jax.shard_map(
        per_device,
        mesh=mesh,
        in_specs=placed,
        out_specs=(
            P(("rep", "fs"), None),
            P(("rep", "fs"), None),
            P("fs", "tp"),
            P("fs", "tp"),
            P("fs", "tp"),
        ),
        check_vma=False,
    )
```

profile of v0, /device:TPU:16, one launch (start us, length us, event | category | flops | bytes accessed | tf_op | source)
XLA Modules:
  0.0 613.5 jit_solution(15810356098618790325)
XLA Ops:
  7.2 0.7 all-gather.7.cloned.1.call-update
  8.0 0.7 all-gather.11.cloned.1.call-update
  8.7 0.0 all-gather.9.cloned.1.call-start
  8.7 0.7 all-gather.9.cloned.1.call-update
  9.4 0.0 all-gather.13.cloned.1.call-start
  9.5 99.6 %all-gather.7.cloned.1.call-done = bf16[2048,1536]{1,0:T(8,128)(2,1)} async-done(((bf16[256,1536]{1,0:T(8,128)(2,1)}), bf16[2048,1536]{1,0:T(8,128)(2,1)}) %all-gather.7.cloned.1.call-update) | async-done | bytes 6291472 | tf_op jit(solution)/shard_map/all_gather | solution.py:31
  109.1 4.0 fusion.10
  113.0 95.1 %all-gather.11.cloned.1.call-done = bf16[2048,1536]{1,0:T(8,128)(2,1)} async-done(((bf16[256,1536]{1,0:T(8,128)(2,1)}), bf16[2048,1536]{1,0:T(8,128)(2,1)}) %all-gather.11.cloned.1.call-update) | async-done | bytes 6291472 | tf_op jit(solution)/shard_map/all_gather | solution.py:33
  208.2 3.8 fusion.9
  211.9 95.3 %all-gather.9.cloned.1.call-done = bf16[2048,1536]{1,0:T(8,128)(2,1)} async-done(((bf16[256,1536]{1,0:T(8,128)(2,1)}), bf16[2048,1536]{1,0:T(8,128)(2,1)}) %all-gather.9.cloned.1.call-update) | async-done | bytes 6291472 | tf_op jit(solution)/shard_map/all_gather | solution.py:32
  307.3 5.1 multiply_convert_fusion
  312.3 0.0 all-gather.15.cloned.1.call-start
  312.4 0.5 all-gather.15.cloned.1.call-update
  312.9 0.0 all-gather.17.cloned.1.call-start
  313.0 0.5 all-gather.17.cloned.1.call-update
  313.5 1.0 copy.26
  314.5 4.8 all-to-all-start
  319.3 1.0 copy.30
  320.3 21.5 %all-to-all-done = bf16[128,8,256]{0,2,1:T(8,128)(2,1)S(1)} async-done(((bf16[128,8,256]{0,2,1:T(8,128)(2,1)}), bf16[128,8,256]{0,2,1:T(8,128)(2,1)S(1)}, u32[]{:S(2)}, u32[]{:S(2)}) %all-to-all-start) | async-done | bytes 524320 | tf_op jit(solution)/shard_map/all_to_all | solution.py:53
  341.9 6.7 %all-to-all-start.1 = ((bf16[128,8,256]{0,2,1:T(8,128)(2,1)}), bf16[128,8,256]{0,2,1:T(8,128)(2,1)S(1)}, u32[]{:S(2)}, u32[]{:S(2)}) async-start(bf16[128,8,256]{0,2,1:T(8,128)(2,1)} %bitcast.5), calls=%async_computation.1 | async-start | bytes 1048576 | tf_op jit(solution)/shard_map/all_to_all | solution.py:54
  348.6 0.2 copy.27
  348.8 22.0 %all-to-all-done.1 = bf16[128,8,256]{0,2,1:T(8,128)(2,1)S(1)} async-done(((bf16[128,8,256]{0,2,1:T(8,128)(2,1)}), bf16[128,8,256]{0,2,1:T(8,128)(2,1)S(1)}, u32[]{:S(2)}, u32[]{:S(2)}) %all-to-all-start.1) | async-done | bytes 524320 | tf_op jit(solution)/shard_map/all_to_all | solution.py:54
  370.8 0.2 copy.31
  371.0 12.0 %all-gather.13.cloned.1.call-done = bf16[1024,1536]{1,0:T(8,128)(2,1)} async-done(((bf16[128,1536]{1,0:T(8,128)(2,1)}), bf16[1024,1536]{1,0:T(8,128)(2,1)}) %all-gather.13.cloned.1.call-update) | async-done | bytes 3145744 | tf_op jit(solution)/shard_map/all_gather | solution.py:56
  383.0 3.8 fusion
  386.8 60.2 %all-gather.15.cloned.1.call-done = bf16[1024,1536]{1,0:T(8,128)(2,1)} async-done(((bf16[128,1536]{1,0:T(8,128)(2,1)}), bf16[1024,1536]{1,0:T(8,128)(2,1)}) %all-gather.15.cloned.1.call-update) | async-done | bytes 3145744 | tf_op jit(solution)/shard_map/all_gather | solution.py:57
  447.0 3.8 fusion.1
  450.8 57.5 %all-gather.17.cloned.1.call-done = bf16[1024,1536]{1,0:T(8,128)(2,1)} async-done(((bf16[128,1536]{1,0:T(8,128)(2,1)}), bf16[1024,1536]{1,0:T(8,128)(2,1)}) %all-gather.17.cloned.1.call-update) | async-done | bytes 3145744 | tf_op jit(solution)/shard_map/all_gather | solution.py:58
  508.3 3.8 fusion.2
  512.2 0.2 all-reduce.5.cloned.1.call-start
  512.4 1.2 copy-done.7
  513.5 1.6 copy.28
  515.2 3.2 copy.32
  518.3 3.0 copy.29
  521.4 5.0 fusion.11
  526.5 1.0 fusion.8
  527.5 0.6 slice-done.3
  528.2 2.9 fusion.3
  531.1 8.8 %convolution_convert_fusion.3 = bf16[128,2048]{1,0:T(8,128)(2,1)} fusion(bf16[2048,1536]{1,0:T(8,128)(2,1)} %all-gather.11.cloned.1.call-done, bf16[128,2048]{1,0:T(8,128)(2,1)S(1)} %copy-done, bf16[2048,1536]{1,0:T(8,128)(2,1)} %all-gather.9.cloned.1.call-done, f32[128,1536]{1,0:T(8,128)S(1)} %fusion.8), kind=kOutput, calls=%fused_computation.10 | convolution fusion | flops 1612054528 | bytes 14417920 | tf_op jit(solution)/shard_map/dot_general | solution.py:8
  539.9 40.2 %all-reduce.7.cloned.1.call-done = (bf16[256,1536]{0,1:T(8,128)(2,1)}, bf16[256,1536]{0,1:T(8,128)(2,1)}, bf16[256,1536]{0,1:T(8,128)(2,1)}) async-done(((bf16[256,1536]{0,1:T(8,128)(2,1)}, bf16[256,1536]{0,1:T(8,128)(2,1)}, bf16[256,1536]{0,1:T(8,128)(2,1)}), (bf16[256,1536]{0,1:T(8,128)(2,1)}, bf16[256,1536]{0,1:T(8,128)(2,1)}, bf16[256,1536]{0,1:T(8,128)(2,1)})) %all-reduce.7.cloned.1.call-update) | async-done | bytes 2359312 | tf_op jit(solution)/shard_map/psum | solution.py:60
  580.1 2.5 convert_add_fusion.2
  582.6 3.1 copy.33
  585.8 3.7 convert_add_fusion
  589.5 3.1 copy.34
  592.6 1.6 copy.35
  594.2 8.7 %all-reduce.5.cloned.1.call-done = (bf16[128,2048]{1,0:T(8,128)(2,1)}, bf16[128,2048]{1,0:T(8,128)(2,1)}) async-done(((bf16[128,2048]{1,0:T(8,128)(2,1)}, bf16[128,2048]{1,0:T(8,128)(2,1)}), (bf16[128,2048]{1,0:T(8,128)(2,1)}, bf16[128,2048]{1,0:T(8,128)(2,1)})) %all-reduce.5.cloned.1.call-update) | async-done | bytes 1048592 | tf_op jit(solution)/shard_map/psum | solution.py:39
  602.9 1.9 copy.41
  604.8 1.9 copy.42
  (34 shorter events, 0.2 us)
Async XLA Ops:
  7.2 519.3 %copy-start = (bf16[128,2048]{1,0:T(8,128)(2,1)S(1)}, bf16[128,2048]{1,0:T(8,128)(2,1)}, u32[]{:S(2)}) copy-start(bf16[128,2048]{1,0:T(8,128)(2,1)} %param.9) | copy-start | bytes 1572868
  7.2 101.9 %all-gather.7.cloned.1.call-start = ((), (), s32[]{:S(2)}) async-start(), calls=%async_computation.2 | async-start | bytes 7077888 | tf_op jit(solution)/shard_map/all_gather | solution.py:31
  7.9 200.2 %all-gather.11.cloned.1.call-start = ((), (), s32[]{:S(2)}) async-start(), calls=%async_computation.4 | async-start | bytes 7077888 | tf_op jit(solution)/shard_map/all_gather | solution.py:33
  8.7 298.6 %all-gather.9.cloned.1.call-start = ((), (), s32[]{:S(2)}) async-start(), calls=%async_computation.3 | async-start | bytes 7077888 | tf_op jit(solution)/shard_map/all_gather | solution.py:32
  9.4 198.8 %copy-start.5 = (bf16[128,2048]{1,0:T(8,128)(2,1)S(1)}, bf16[128,2048]{1,0:T(8,128)(2,1)}, u32[]{:S(2)}) copy-start(bf16[128,2048]{1,0:T(8,128)(2,1)} %param.11) | copy-start | bytes 1572868
  9.4 373.6 %all-gather.13.cloned.1.call-start = ((), (), s32[]{:S(2)}) async-start(), calls=%async_computation.5 | async-start | bytes 3538944 | tf_op jit(solution)/shard_map/all_gather | solution.py:56
  113.0 194.2 %copy-start.4 = (bf16[128,2048]{1,0:T(8,128)(2,1)S(1)}, bf16[128,2048]{1,0:T(8,128)(2,1)}, u32[]{:S(2)}) copy-start(bf16[128,2048]{1,0:T(8,128)(2,1)} %param.10) | copy-start | bytes 1572868
  312.3 134.6 %all-gather.15.cloned.1.call-start = ((), (), s32[]{:S(2)}) async-start(), calls=%async_computation.6 | async-start | bytes 3538944 | tf_op jit(solution)/shard_map/all_gather | solution.py:57
  312.9 195.4 %all-gather.17.cloned.1.call-start = ((), (), s32[]{:S(2)}) async-start(), calls=%async_computation.7 | async-start | bytes 3538944 | tf_op jit(solution)/shard_map/all_gather | solution.py:58
  314.5 27.4 %all-to-all-start = ((bf16[128,8,256]{0,2,1:T(8,128)(2,1)}), bf16[128,8,256]{0,2,1:T(8,128)(2,1)S(1)}, u32[]{:S(2)}, u32[]{:S(2)}) async-start(bf16[128,8,256]{0,2,1:T(8,128)(2,1)} %bitcast), calls=%async_computation | async-start | bytes 1048576 | tf_op jit(solution)/shard_map/all_to_all | solution.py:53
  341.9 28.9 %all-to-all-start.1 = ((bf16[128,8,256]{0,2,1:T(8,128)(2,1)}), bf16[128,8,256]{0,2,1:T(8,128)(2,1)S(1)}, u32[]{:S(2)}, u32[]{:S(2)}) async-start(bf16[128,8,256]{0,2,1:T(8,128)(2,1)} %bitcast.5), calls=%async_computation.1 | async-start | bytes 1048576 | tf_op jit(solution)/shard_map/all_to_all | solution.py:54
  348.6 231.6 %all-reduce.7.cloned.1.call-start = ((), (), s32[]{:S(2)}) async-start(), calls=%async_computation.9 | async-start | bytes 4718592 | tf_op jit(solution)/shard_map/psum | solution.py:60
  512.1 1.4 copy-start.7
  512.2 90.7 %all-reduce.5.cloned.1.call-start = ((), (), s32[]{:S(2)}) async-start(), calls=%async_computation.8 | async-start | bytes 2097152 | tf_op jit(solution)/shard_map/psum | solution.py:39
  515.2 6.2 %copy-start.8 = (bf16[128,1536]{1,0:T(8,128)(2,1)S(1)}, bf16[128,1536]{1,0:T(8,128)(2,1)}, u32[]{:S(2)}) copy-start(bf16[128,1536]{1,0:T(8,128)(2,1)} %get-tuple-element.26) | copy-start | bytes 1179652
  515.2 11.3 %slice-start = ((s8[6291456]{0:T(1024)(128)(4,1)}), s8[2097152]{0:T(1024)(128)(4,1)S(1)}, s32[]{:S(2)}) async-start(s8[6291456]{0:T(1024)(128)(4,1)} %bitcast.33), calls=%async_computation.10 | async-start | bytes 4194304
  521.4 5.1 slice-start.1
  521.4 6.1 slice-start.2
  526.5 1.7 slice-start.3
  526.5 1.7 copy-start.6
  531.1 49.0 %copy-start.1 = (f32[256,1536]{0,1:T(8,128)S(1)}, f32[256,1536]{0,1:T(8,128)}, u32[]{:S(2)}) copy-start(f32[256,1536]{0,1:T(8,128)} %copy.28) | copy-start | bytes 4718596
  580.1 5.6 copy-start.9
  582.6 3.1 copy-start.2
  589.5 3.2 copy-start.3
Sparse Core Ops, SparseCore 0:
  10.2 98.8 all-gather.6
  111.2 96.8 all-gather.10
  210.3 96.8 all-gather.8
  312.5 70.5 all-gather.12
  385.1 61.8 all-gather.14
  449.6 58.6 all-gather.16
  512.3 67.7 all-reduce.6
  583.1 19.7 all-reduce.4
where the time goes:
time: 616 us; the launch traced here: 614 us
  waiting for transfers between devices  515 us (84%)
  matrix products  42 us (7%)
  local copies, waits for them, and re-layouts  23.8 us (4%)
  between operations  14.3 us (2%)
  starting transfers between devices  12 us (2%)
  other arithmetic  6.18 us (1%)
    all_gather x1, waiting for transfers between devices, per_device(): lax.all_gather(gate_weight, 'fs', axis=0, tiled=True)  99.6 us
    all_gather x1, waiting for transfers between devices, per_device(): lax.all_gather(up_weight, 'fs', axis=0, tiled=True)  95.3 us
    all_gather x1, waiting for transfers between devices, per_device(): lax.all_gather(down_weight, 'fs', axis=0, tiled=True)  95.1 us
    all_gather x1, waiting for transfers between devices, per_device(): lax.all_gather(up_grad, 'fs', axis=0, tiled=True)  60.2 us
    all_gather x1, waiting for transfers between devices, per_device(): lax.all_gather(hidden_early, 'fs', axis=0, tiled=True)  57.5 us
    psum x1, waiting for transfers between devices, per_device(): lax.psum(gate_local.astype(jnp.bfloat16), 'rep').astype(jnp.float32)  40.2 us
    unnamed x38, local copies, waits for them, and re-layouts  23.3 us
    all_to_all x1, waiting for transfers between devices, per_device(): lax.all_to_all(cotangent, 'fs', split_axis=1, concat_axis=0, tiled=True)  22 us
  transfers between devices with their start and end apart: 10, of which 10 were waited for; matrix products, arithmetic and copies ran while one was open for 9% of the time, Pallas kernels for 0%

commit v1 on v0

--- a/solution.py
+++ b/solution.py
@@ -1,7 +1,306 @@
+import functools
+
 import jax
 import jax.numpy as jnp
 from jax import lax
+from jax.experimental import pallas as pl
+from jax.experimental.pallas import tpu as pltpu
 from jax.sharding import PartitionSpec as P
+
+MESH = pl.DeviceIdType.MESH
+
+
+def ring_position(index, n):
+    side, height = lax.rem(index, 2), index // 2
+    return (1 - side) * height + side * (n - 1 - height)
+
+
+def ring_index(position, n):
+    position = lax.rem(position + 2 * n, n)
+    back = position // (n // 2)
+    return (1 - back) * (2 * position) + back * (2 * (n - 1 - position) + 1)
+
+
+def span(start, size, step):
+    return pl.ds(pl.multiple_of(start, step), size)
+
+
+def remote(source, target, send, recv, device):
+    return pltpu.make_async_remote_copy(
+        src_ref=source,
+        dst_ref=target,
+        send_sem=send,
+        recv_sem=recv,
+        device_id=device,
+        device_id_type=MESH,
+    )
+
+
+def meet(n, r, f, t):
+    barrier = pltpu.get_barrier_semaphore()
+    for k in range(1, n):
+        pl.semaphore_signal(barrier, inc=1, device_id={"fs": lax.rem(f + k, n)}, device_id_type=MESH)
+    pl.semaphore_signal(barrier, inc=1, device_id={"rep": 1 - r}, device_id_type=MESH)
+    pl.semaphore_signal(barrier, inc=1, device_id={"tp": 1 - t}, device_id_type=MESH)
+    pl.semaphore_wait(barrier, n + 1)
+
+
+def gather_kernel(n, tok, wt, tok_out, w_out, rs, rr, ps, pr, ws, wr, xs, xr):
+    r, f, t = lax.axis_index("rep"), lax.axis_index("fs"), lax.axis_index("tp")
+    m = tok.shape[1]
+    q = m // 4
+    hid, dl = wt.shape[1] // n, wt.shape[2]
+    hl = dl // 2
+    pos = ring_position(f, n)
+    ahead = (ring_index(pos + 1, n), ring_index(pos - 1, n))
+    meet(n, r, f, t)
+
+    def rows(origin, core, d):
+        return tok_out.at[:, span(origin * m + core * (2 * q) + d * q, q, q), :]
+
+    def piece(origin, part):
+        return w_out.at[:, :, span(origin * dl + part * hl, hl, hl)]
+
+    pending = []
+    for d in range(2):
+        copy = remote(
+            tok.at[:, span(t * (2 * q) + d * q, q, q), :],
+            rows(f, t, d), rs.at[d, 0], rr.at[d, 0], {"fs": ahead[d]},
+        )
+        copy.start()
+        pending.append(copy)
+    for k in range(1, n):
+        g = lax.rem(f + k, n)
+        copy = remote(
+            wt.at[:, span(g * hid, hid, hid), span(r * hl, hl, hl)],
+            piece(f, r), ws.at[k - 1], wr.at[k - 1], {"fs": g},
+        )
+        copy.start()
+        pending.append(copy)
+    tok_out[:, span(f * m, m, m), :] = tok[...]
+    w_out[:, :, span(f * dl, dl, dl)] = wt[:, span(f * hid, hid, hid), :]
+
+    arrivals = []
+    for s in range(1, n):
+        for d in range(2):
+            origin = ring_index(pos - s if d == 0 else pos + s, n)
+            block = rows(origin, t, d)
+            remote(block, block, rs.at[d, s - 1], rr.at[d, s - 1], {"fs": ahead[d]}).wait_recv()
+            if s < n - 1:
+                copy = remote(block, block, rs.at[d, s], rr.at[d, s], {"fs": ahead[d]})
+                copy.start()
+                pending.append(copy)
+            copy = remote(block, block, ps.at[d, s - 1], pr.at[d, s - 1], {"tp": 1 - t})
+            copy.start()
+            pending.append(copy)
+            other = rows(origin, 1 - t, d)
+            arrivals.append(remote(other, other, ps.at[d, s - 1], pr.at[d, s - 1], {"tp": 1 - t}))
+        origin = lax.rem(f - s + n, n)
+        block = piece(origin, r)
+        remote(block, block, ws.at[s - 1], wr.at[s - 1], {"fs": origin}).wait_recv()
+        copy = remote(block, block, xs.at[s - 1], xr.at[s - 1], {"rep": 1 - r})
+        copy.start()
+        pending.append(copy)
+        other = piece(origin, 1 - r)
+        arrivals.append(remote(other, other, xs.at[s - 1], xr.at[s - 1], {"rep": 1 - r}))
+    for copy in arrivals:
+        copy.wait_recv()
+    for copy in pending:
+        copy.wait_send()
+
+
+def scatter_kernel(
+    n, late, early, grads, late_out, early_out, g_out,
+    peer, ring_in, ring_out, x_in, x_out,
+    ts, tr, rs, rr, os_, or_, xs, xr, gs, gr, fs_, fr,
+):
+    r, f, t = lax.axis_index("rep"), lax.axis_index("fs"), lax.axis_index("tp")
+    m = late.shape[1]
+    q = m // 4
+    hid = grads.shape[1]
+    dl = grads.shape[2] // n
+    hl = dl // 2
+    pos = ring_position(f, n)
+    ahead = (ring_index(pos + 1, n), ring_index(pos - 1, n))
+    parts, outs = (late, early), (late_out, early_out)
+    f32 = jnp.float32
+    meet(n, r, f, t)
+
+    pending = []
+
+    def go(copy):
+        copy.start()
+        pending.append(copy)
+
+    for o in range(2):
+        go(remote(parts[o].at[:, span((1 - t) * (2 * q), 2 * q, 2 * q), :], peer.at[o], ts.at[o], tr.at[o], {"tp": 1 - t}))
+    order = list(range(1, n)) + [0]
+    for k in order:
+        g = lax.rem(f + k, n)
+        go(remote(grads.at[:, :, span(g * dl + (1 - r) * hl, hl, hl)], x_in.at[k], xs.at[k], xr.at[k], {"rep": 1 - r}))
+
+    def own(o, b, d):
+        return (
+            parts[o][b, span(t * (2 * q) + d * q, q, q), :].astype(f32)
+            + peer[o, b, d * q:(d + 1) * q, :].astype(f32)
+        )
+
+    def g_block(origin, part):
+        return g_out.at[:, span(origin * hid, hid, hid), span(part * hl, hl, hl)]
+
+    def pair_sum(k):
+        g = lax.rem(f + k, n)
+        remote(x_in.at[k], x_in.at[k], xs.at[k], xr.at[k], {"rep": 1 - r}).wait_recv()
+        return (x_in[k].astype(f32) + grads[:, :, span(g * dl + r * hl, hl, hl)].astype(f32)).astype(jnp.bfloat16)
+
+    def pass_on(k):
+        origin = lax.rem(f - k + n, n)
+        block = g_block(origin, r)
+        remote(block, block, gs.at[k - 1], gr.at[k - 1], {"fs": origin}).wait_recv()
+        go(remote(block, block, fs_.at[k], fr.at[k], {"rep": 1 - r}))
+
+    for s in range(n - 1):
+        for o in range(2):
+            if s == 0:
+                remote(peer.at[o], peer.at[o], ts.at[o], tr.at[o], {"tp": 1 - t}).wait_recv()
+            for d in range(2):
+                b = ring_index(pos - 1 - s if d == 0 else pos + 1 + s, n)
+                value = own(o, b, d)
+                if s > 0:
+                    slot = ring_in.at[d, s - 1, o]
+                    remote(slot, slot, rs.at[d, s - 1, o], rr.at[d, s - 1, o], {"fs": ahead[d]}).wait_recv()
+                    value = value + ring_in[d, s - 1, o].astype(f32)
+                ring_out[d, s, o] = value.astype(jnp.bfloat16)
+                go(remote(ring_out.at[d, s, o], ring_in.at[d, s, o], rs.at[d, s, o], rr.at[d, s, o], {"fs": ahead[d]}))
+        x_out[s] = pair_sum(s + 1)
+        go(remote(x_out.at[s], g_block(f, r), gs.at[s], gr.at[s], {"fs": lax.rem(f + s + 1, n)}))
+        if s >= 2:
+            pass_on(s - 1)
+    g_out[:, span(f * hid, hid, hid), span(r * hl, hl, hl)] = pair_sum(0)
+    block = g_block(f, r)
+    go(remote(block, block, fs_.at[0], fr.at[0], {"rep": 1 - r}))
+    for o in range(2):
+        for d in range(2):
+            slot = ring_in.at[d, n - 2, o]
+            remote(slot, slot, rs.at[d, n - 2, o], rr.at[d, n - 2, o], {"fs": ahead[d]}).wait_recv()
+            value = own(o, f, d) + ring_in[d, n - 2, o].astype(f32)
+            outs[o][span(t * (2 * q) + d * q, q, q), :] = value.astype(jnp.bfloat16)
+        half = outs[o].at[span(t * (2 * q), 2 * q, 2 * q), :]
+        go(remote(half, half, os_.at[o], or_.at[o], {"tp": 1 - t}))
+    for k in range(n - 2, n):
+        pass_on(k)
+    for o in range(2):
+        half = outs[o].at[span((1 - t) * (2 * q), 2 * q, 2 * q), :]
+        remote(half, half, os_.at[o], or_.at[o], {"tp": 1 - t}).wait_recv()
+    for k in range(n):
+        block = g_block(lax.rem(f - k + n, n), 1 - r)
+        remote(block, block, fs_.at[k], fr.at[k], {"rep": 1 - r}).wait_recv()
+    for copy in pending:
+        copy.wait_send()
+
+
+VMEM = pl.BlockSpec(memory_space=pltpu.VMEM)
+
+
+def dma(*shape):
+    return pltpu.SemaphoreType.DMA(shape)
+
+
+def split_hidden(
+    n,
+    later_input,
+    earlier_input,
+    cotangent,
+    gate_weight,
+    up_weight,
+    down_weight,
+    gate_sum,
+    up_sum,
+    down_sum,
+):
+    bf16 = jnp.bfloat16
+    m, width = later_input.shape
+    dl, ff = gate_weight.shape
+    hid = ff // n
+    hl, q = dl // 2, m // 4
+    tokens = jnp.stack([later_input, earlier_input, cotangent])
+    weights = jnp.stack([gate_weight.T, up_weight.T, down_weight.T])
+    tok, w = pl.pallas_call(
+        functools.partial(gather_kernel, n),
+        out_shape=(
+            jax.ShapeDtypeStruct((3, n * m, width), bf16),
+            jax.ShapeDtypeStruct((3, hid, width), bf16),
+        ),
+        in_specs=[VMEM] * 2,
+        out_specs=(VMEM, VMEM),
+        scratch_shapes=[dma(2, n - 1)] * 4 + [dma(n - 1)] * 4,
+        compiler_params=pltpu.CompilerParams(
+            collective_id=0, has_side_effects=True, vmem_limit_bytes=60 * 1024 * 1024
+        ),
+        name="gather",
+    )(tokens, weights)
+    count = n * m
+    both = tok[:2].reshape(2 * count, width)
+    gate, up = contract_last(both, w[0]), contract_last(both, w[1])
+    hidden_late = (jax.nn.silu(gate[:count]) * up[:count]).astype(bf16)
+    late = jnp.dot(hidden_late, w[2], preferred_element_type=jnp.float32).astype(bf16)
+    gate_early, up_early = gate[count:], up[count:]
+    hidden_grad = contract_last(tok[2], w[2])
+    gate_grad, up_grad, hidden_early = early_parts(gate_early, up_early, hidden_grad)
+    early = (
+        jnp.dot(gate_grad, w[0], preferred_element_type=jnp.float32)
+        + jnp.dot(up_grad, w[1], preferred_element_type=jnp.float32)
+    ).astype(bf16)
+    grads = jnp.stack([
+        contract_first(gate_grad, tok[1]).astype(bf16),
+        contract_first(up_grad, tok[1]).astype(bf16),
+        contract_first(hidden_early, tok[2]).astype(bf16),
+    ])
+    later_output, earlier_input_grad, total = pl.pallas_call(
+        functools.partial(scatter_kernel, n),
+        out_shape=(
+            jax.ShapeDtypeStruct((m, width), bf16),
+            jax.ShapeDtypeStruct((m, width), bf16),
+            jax.ShapeDtypeStruct((3, ff, dl), bf16),
+        ),
+        in_specs=[VMEM] * 3,
+        out_specs=(VMEM, VMEM, VMEM),
+        scratch_shapes=[
+            pltpu.VMEM((2, n, 2 * q, width), bf16),
+            pltpu.VMEM((2, n - 1, 2, q, width), bf16),
+            pltpu.VMEM((2, n - 1, 2, q, width), bf16),
+            pltpu.VMEM((n, 3, hid, hl), bf16),
+            pltpu.VMEM((n - 1, 3, hid, hl), bf16),
+            dma(2), dma(2),
+            dma(2, n - 1, 2), dma(2, n - 1, 2),
+            dma(2), dma(2),
+            dma(n), dma(n),
+            dma(n - 1), dma(n - 1),
+            dma(n), dma(n),
+        ],
+        compiler_params=pltpu.CompilerParams(
+            collective_id=1, has_side_effects=True, vmem_limit_bytes=60 * 1024 * 1024
+        ),
+        name="scatter",
+    )(late.reshape(n, m, width), early.reshape(n, m, width), grads)
+    return (
+        later_output,
+        earlier_input_grad,
+        gate_sum + total[0].T.astype(jnp.float32),
+        up_sum + total[1].T.astype(jnp.float32),
+        down_sum + total[2].T.astype(jnp.float32),
+    )
+
+
+def early_parts(gate_early, up_early, hidden_grad):
+    sigmoid_gate = jax.nn.sigmoid(gate_early)
+    silu_early = gate_early * sigmoid_gate
+    gate_grad = (
+        hidden_grad * up_early * sigmoid_gate * (1.0 + gate_early * (1.0 - sigmoid_gate))
+    ).astype(jnp.bfloat16)
+    up_grad = (hidden_grad * silu_early).astype(jnp.bfloat16)
+    hidden_early = (silu_early * up_early).astype(jnp.bfloat16)
+    return gate_grad, up_grad, hidden_early
 
 
 def contract_last(first, second):
@@ -82,8 +381,23 @@
         P("fs", "tp"),
         P("fs", "tp"),
     )
+    reps, shards, blocks = (mesh.shape[axis] for axis in ("rep", "fs", "tp"))
+
+    def chosen(*arrays):
+        rows = arrays[0].shape[0]
+        depth, units = arrays[3].shape
+        fits = (
+            reps == 2
+            and blocks == 2
+            and shards % 2 == 0
+            and units % (shards * 16) == 0
+            and depth % 256 == 0
+            and rows % 64 == 0
+        )
+        return split_hidden(shards, *arrays) if fits else per_device(*arrays)
+
     return jax.shard_map(
-        per_device,
+        chosen,
         mesh=mesh,
         in_specs=placed,
         out_specs=(

time: 616 us -> 246 us (0.40)
  waiting for transfers between devices: 515 us -> 0 us
  Pallas kernels: 0 us -> 189 us
  matrix products: 42 us -> 22.2 us
  between operations: 14.3 us -> 0.82 us
  starting transfers between devices: 12 us -> 0 us
    all_gather x6 -> x0, waiting for transfers between devices: 420 us -> none  [the longest x1 99.6 us: per_device(): lax.all_gather(gate_weight, 'fs', axis=0, tiled=True)]
    pallas_call x0 -> x2, Pallas kernels: none -> 189 us  [the longest x1 102 us: split_hidden(): pl.pallas_call(functools.partial(gather_kernel, n), out_shape=(jax.ShapeD...]
    psum x2 -> x0, waiting for transfers between devices: 48.9 us -> none  [the longest x1 40.2 us: per_device(): lax.psum(gate_local.astype(jnp.bfloat16), 'rep').astype(jnp.float32)]
    all_to_all x2 -> x0, waiting for transfers between devices: 43.5 us -> none  [the longest x1 22 us: per_device(): lax.all_to_all(cotangent, 'fs', split_axis=1, concat_axis=0, tiled=True)]
    all_to_all x2 -> x0, starting transfers between devices: 11.5 us -> none  [the longest x1 6.69 us: per_device(): lax.all_to_all(cotangent, 'fs', split_axis=1, concat_axis=0, tiled=True)]
    dot_general x3, matrix products: 11.5 us -> 3.06 us  [contract_first(): lax.dot_general(first, second, (((0,), (0,)), ((), ())), preferred_elemen...]
    slice x0 -> x1, local copies, waits for them, and re-layouts: none -> 8.39 us  [split_hidden(): both = tok[:2].reshape(2 * count, width)]
    unnamed x38 -> x39, local copies, waits for them, and re-layouts: 23.3 us -> 16.1 us
  transfers between devices with their start and end apart: 10 -> 0, of which waited for: 10 -> 0; matrix products, arithmetic and copies ran while one was open for 9% -> 0% of each run, Pallas kernels for 0% -> 0%
where the time goes in v1:
time: 246 us
  Pallas kernels  189 us (77%)
  local copies, waits for them, and re-layouts  24.5 us (10%)
  matrix products  22.2 us (9%)
  other arithmetic  9.41 us (4%)
    pallas_call x1, Pallas kernels, split_hidden(): pl.pallas_call(functools.partial(gather_kernel, n), out_shape=(jax.ShapeD...  102 us
    pallas_call x1, Pallas kernels, split_hidden(): pl.pallas_call(functools.partial(scatter_kernel, n), out_shape=(jax.Shape...  87.2 us
    unnamed x39, local copies, waits for them, and re-layouts  16.1 us
    dot_general x3, matrix products, contract_last(): lax.dot_general(first, second, (((1,), (1,)), ((), ())), preferred_elemen...  11.1 us
    slice x1, local copies, waits for them, and re-layouts, split_hidden(): both = tok[:2].reshape(2 * count, width)  8.39 us

profile of v1, /device:TPU:16, one launch (start us, length us, event | category | flops | bytes accessed | tf_op | source)
XLA Modules:
  0.0 245.8 jit_solution(2634301881737948747)
XLA Ops:
  0.6 0.0 copy-start.5
  0.6 1.5 copy.14
  2.1 1.4 copy.15
  3.5 0.0 copy-done.5
  3.5 0.3 copy.16
  3.8 0.0 copy-start.8
  3.8 0.0 copy-start.9
  3.8 0.0 copy-start.10
  3.9 1.7 pad_maximum_fusion.wt
  5.5 0.0 copy-done.8
  5.5 0.0 copy-done.9
  5.5 0.1 copy-done.10
  5.6 1.3 pad_maximum_fusion.2.tok
  6.9 101.6 %gather.1 = (bf16[3,1024,2048]{2,1,0:T(8,128)(2,1)}, bf16[3,192,2048]{2,1,0:T(8,128)(2,1)}) custom-call(bf16[3,128,2048]{2,1,0:T(8,128)(2,1)} %pad_maximum_fusion.2.tok, bf16[3,1536,256]{2,1,0:T(8,128)(2,1)} %pad_maximum_fusion.wt), custom_call_target="tpu_custom_call" | custom-call | tf_op jit(solution)/shard_map/gather/pallas_call | solution.py:228
  108.5 0.0 copy-start.4
  108.5 8.4 %slice.44 = bf16[2,1024,2048]{2,1,0:T(8,128)(2,1)} slice(bf16[3,1024,2048]{2,1,0:T(8,128)(2,1)} %get-tuple-element.10), slice={[0:2], [0:1024], [0:2048]} | slice | bytes 16777216 | tf_op jit(solution)/shard_map/slice | solution.py:243
  116.9 0.0 copy-done.4
  116.9 6.4 %fusion.41 = f32[2048,192]{0,1:T(8,128)S(1)} fusion(bf16[2048,2048]{1,0:T(8,128)(2,1)} %bitcast.90, bf16[3,192,2048]{2,1,0:T(8,128)(2,1)S(1)} %copy-done.4), kind=kOutput, calls=%fused_computation.38 | convolution fusion | flops 1610612736 | bytes 10747904 | tf_op jit(solution)/shard_map/dot_general | solution.py:307
  123.3 0.0 copy-done
  123.3 0.0 slice-start.2
  123.4 2.9 %fusion.37 = f32[2048,192]{0,1:T(8,128)S(1)} fusion(bf16[2048,2048]{1,0:T(8,128)(2,1)S(1)} %bitcast.91, bf16[3,192,2048]{2,1,0:T(8,128)(2,1)S(1)} %copy-done.4), kind=kOutput, calls=%fused_computation.34 | convolution fusion | flops 1610612736 | bytes 10747904 | tf_op jit(solution)/shard_map/dot_general | solution.py:307
  126.3 0.0 slice-done
  126.3 0.0 slice-done.1
  126.3 0.2 slice-done.2
  126.5 1.8 multiply_convert_fusion.1
  128.2 1.0 fusion.24
  129.3 1.0 fusion.21
  130.3 1.0 fusion.27
  131.3 1.7 pad_maximum_fusion.1.grads
  133.1 1.5 fusion.39
  134.6 3.3 %add_convert_fusion = bf16[1024,2048]{1,0:T(8,128)(2,1)} fusion(f32[1024,2048]{1,0:T(8,128)S(1)} %fusion.39, bf16[1024,192]{0,1:T(8,128)(2,1)S(1)} %get-tuple-element.23, bf16[3,192,2048]{2,1,0:T(8,128)(2,1)S(1)} %copy-done.4), kind=kOutput, calls=%fused_computation | convolution fusion | flops 809500672 | bytes 13762560 | tf_op jit(solution)/shard_map/dot_general | solution.py:252
  137.9 3.3 %convolution_convert_fusion = bf16[1024,2048]{1,0:T(8,128)(2,1)} fusion(bf16[3,192,2048]{2,1,0:T(8,128)(2,1)S(1)} %copy-done.4, f32[2048,192]{0,1:T(8,128)S(1)} %fusion.37, f32[2048,192]{0,1:T(8,128)S(1)} %fusion.41), kind=kOutput, calls=%fused_computation.9 | convolution fusion | flops 808583168 | bytes 6553600 | tf_op jit(solution)/shard_map/dot_general | solution.py:246
  141.1 87.2 %scatter.1 = (bf16[128,2048]{1,0:T(8,128)(2,1)}, bf16[128,2048]{1,0:T(8,128)(2,1)}, bf16[3,1536,256]{2,1,0:T(8,128)(2,1)}) custom-call(bf16[8,128,2048]{2,1,0:T(8,128)(2,1)} %bitcast.94, bf16[8,128,2048]{2,1,0:T(8,128)(2,1)} %bitcast.89, bf16[3,192,2048]{2,1,0:T(8,128)(2,1)} %pad_maximum_fusion.1.grads), custom_call_target="tpu_custom_call" | custom-call | tf_op jit(solution)/shard_map/scatter/pallas_call | solution.py:259
  228.3 0.0 copy-start.2
  228.4 0.0 copy-done.1
  228.4 1.6 copy.17
  230.0 0.0 copy-done.2
  230.0 1.6 copy.18
  231.6 0.0 copy-done.3
  231.6 1.6 copy.19
  233.2 4.7 %fusion.30 = (f32[256,1536]{0,1:T(8,128)S(1)}, f32[256,1536]{0,1:T(8,128)S(1)}, f32[256,1536]{0,1:T(8,128)}) fusion(f32[256,1536]{0,1:T(8,128)} %copy.19, bf16[3,1536,256]{2,1,0:T(8,128)(2,1)} %get-tuple-element.14, f32[256,1536]{0,1:T(8,128)} %copy.18, f32[256,1536]{0,1:T(8,128)} %copy.17), kind=kLoop, calls=%fused_computation.24 | loop fusion | flops 2359296 | bytes 11796480 | tf_op jit(solution)/shard_map/add | solution.py:291
  237.9 3.0 %copy.20 = f32[256,1536]{1,0:T(8,128)} copy(f32[256,1536]{0,1:T(8,128)} %get-tuple-element.22) | data formatting | bytes 3145728
  240.9 1.6 copy.21
  242.5 1.6 copy.22
  244.2 0.0 copy-done.7
  244.2 0.8 copy.25
  245.0 0.0 copy-done.6
  245.0 0.8 copy.26
  (8 shorter events, 0.0 us)
Async XLA Ops:
  0.6 2.9 %copy-start.5 = (bf16[256,1536]{1,0:T(8,128)(2,1)S(1)}, bf16[256,1536]{1,0:T(8,128)(2,1)}, u32[]{:S(2)}) copy-start(bf16[256,1536]{1,0:T(8,128)(2,1)} %param.14) | copy-start | bytes 2359300
  3.8 1.7 copy-start.8
  3.8 1.7 copy-start.9
  3.8 1.7 copy-start.10
  108.5 8.4 %copy-start.4 = (bf16[3,192,2048]{2,1,0:T(8,128)(2,1)S(1)}, bf16[3,192,2048]{2,1,0:T(8,128)(2,1)}, u32[]{:S(2)}) copy-start(bf16[3,192,2048]{2,1,0:T(8,128)(2,1)} %get-tuple-element.11) | copy-start | bytes 7077892
  116.9 6.5 %copy-start = (bf16[2,1024,2048]{2,1,0:T(8,128)(2,1)S(1)}, bf16[2,1024,2048]{2,1,0:T(8,128)(2,1)}, u32[]{:S(2)}) copy-start(bf16[2,1024,2048]{2,1,0:T(8,128)(2,1)} %slice.44) | copy-start | bytes 25165828
  116.9 9.4 %slice-start = ((s8[12582912]{0:T(1024)(128)(4,1)}), s8[4194304]{0:T(1024)(128)(4,1)S(1)}, s32[]{:S(2)}) async-start(s8[12582912]{0:T(1024)(128)(4,1)} %bitcast.92), calls=%async_computation | async-start | bytes 8388608
  116.9 9.4 %slice-start.1 = ((s8[12582912]{0:T(1024)(128)(4,1)}), s8[4194304]{0:T(1024)(128)(4,1)S(1)}, s32[]{:S(2)}) async-start(s8[12582912]{0:T(1024)(128)(4,1)} %bitcast.92), calls=%async_computation.1 | async-start | bytes 8388608
  123.3 3.1 %slice-start.2 = ((s8[12582912]{0:T(1024)(128)(4,1)}), s8[4194304]{0:T(1024)(128)(4,1)S(1)}, s32[]{:S(2)}) async-start(s8[12582912]{0:T(1024)(128)(4,1)} %bitcast.92), calls=%async_computation.2 | async-start | bytes 8388608
  141.1 87.2 %copy-start.1 = (f32[256,1536]{1,0:T(8,128)S(1)}, f32[256,1536]{1,0:T(8,128)}, u32[]{:S(2)}) copy-start(f32[256,1536]{1,0:T(8,128)} %param.15) | copy-start | bytes 4718596
  228.3 1.6 copy-start.2
  230.0 1.6 copy-start.3
  242.5 1.6 copy-start.7
  242.5 2.4 copy-start.6

commit v2 on v1

v2 whole, which is shorter than its diff:
```python
import functools

import jax
import jax.numpy as jnp
from jax import lax
from jax.experimental import pallas as pl
from jax.experimental.pallas import tpu as pltpu
from jax.sharding import PartitionSpec as P

MESH = pl.DeviceIdType.MESH


def ring_position(index, n):
    side, height = lax.rem(index, 2), index // 2
    return (1 - side) * height + side * (n - 1 - height)


def ring_index(position, n):
    position = lax.rem(position + 2 * n, n)
    back = position // (n // 2)
    return (1 - back) * (2 * position) + back * (2 * (n - 1 - position) + 1)


def span(start, size, step):
    return pl.ds(pl.multiple_of(start, step), size)


def remote(source, target, send, recv, device):
    return pltpu.make_async_remote_copy(
        src_ref=source,
        dst_ref=target,
        send_sem=send,
        recv_sem=recv,
        device_id=device,
        device_id_type=MESH,
    )


def meet(n, r, f, t):
    barrier = pltpu.get_barrier_semaphore()
    for k in range(1, n):
        pl.semaphore_signal(barrier, inc=1, device_id={"fs": lax.rem(f + k, n)}, device_id_type=MESH)
    pl.semaphore_signal(barrier, inc=1, device_id={"rep": 1 - r}, device_id_type=MESH)
    pl.semaphore_signal(barrier, inc=1, device_id={"tp": 1 - t}, device_id_type=MESH)
    pl.semaphore_wait(barrier, n + 1)


def fused_kernel(
    n, tok, wt, late_out, early_out, g_out,
    slots, w, part, peer, acc, grads, ring_in, ring_out, x_in, x_out,
    ags, agr, aps, apr, ws, wr, wxs, wxr,
    ts, tr, rs, rr, os_, or_, xs, xr, gs, gr, fs_, fr,
):
    r, f, t = lax.axis_index("rep"), lax.axis_index("fs"), lax.axis_index("tp")
    m = tok.shape[1]
    q = m // 4
    hid, dl = wt.shape[1] // n, wt.shape[2]
    hl = dl // 2
    width = tok.shape[2]
    pos = ring_position(f, n)
    ahead = (ring_index(pos + 1, n), ring_index(pos - 1, n))
    outs = (late_out, early_out)
    f32, bf16 = jnp.float32, jnp.bfloat16
    meet(n, r, f, t)

    pending = []

    def go(copy):
        copy.start()
        pending.append(copy)

    def quarter(core, d):
        return span(core * (2 * q) + d * q, q, q)

    def half(core):
        return span(core * (2 * q), 2 * q, 2 * q)

    def piece(origin, side):
        return w.at[:, :, span(origin * dl + side * hl, hl, hl)]

    for k in range(1, n):
        g = lax.rem(f + k, n)
        go(remote(
            wt.at[:, span(g * hid, hid, hid), span(r * hl, hl, hl)],
            piece(f, r), ws.at[k - 1], wr.at[k - 1], {"fs": g},
        ))
    for d in range(2):
        go(remote(tok.at[:, quarter(t, d), :], slots.at[1, :, quarter(t, d), :], ags.at[d, 0], agr.at[d, 0], {"fs": ahead[d]}))
    slots[0] = tok[...]
    w[:, :, span(f * dl, dl, dl)] = wt[:, span(f * hid, hid, hid), :]
    acc[...] = jnp.zeros_like(acc)
    for k in range(1, n):
        origin = lax.rem(f - k + n, n)
        block = piece(origin, r)
        remote(block, block, ws.at[k - 1], wr.at[k - 1], {"fs": origin}).wait_recv()
        go(remote(block, block, wxs.at[k - 1], wxr.at[k - 1], {"rep": 1 - r}))
    for k in range(1, n):
        block = piece(lax.rem(f - k + n, n), 1 - r)
        remote(block, block, wxs.at[k - 1], wxr.at[k - 1], {"rep": 1 - r}).wait_recv()

    step = width // 4

    def compute(s):
        pair = slots[s, 0:2].reshape(2 * m, width)
        gate, up = contract_last(pair, w[0]), contract_last(pair, w[1])
        hidden_late = (jax.nn.silu(gate[:m]) * up[:m]).astype(bf16)
        hidden_grad = contract_last(slots[s, 2], w[2])
        gate_grad, up_grad, hidden_early = early_parts(gate[m:], up[m:], hidden_grad)
        for c in range(4):
            lanes = slice(c * step, (c + 1) * step)
            part[s, 0, :, lanes] = jnp.dot(hidden_late, w[2, :, lanes], preferred_element_type=f32).astype(bf16)
            part[s, 1, :, lanes] = (
                jnp.dot(gate_grad, w[0, :, lanes], preferred_element_type=f32)
                + jnp.dot(up_grad, w[1, :, lanes], preferred_element_type=f32)
            ).astype(bf16)
            early = slots[s, 1, :, lanes]
            acc[0, :, lanes] += contract_first(gate_grad, early)
            acc[1, :, lanes] += contract_first(up_grad, early)
            acc[2, :, lanes] += contract_first(hidden_early, slots[s, 2, :, lanes])

    def trade(s):
        return remote(part.at[s, :, half(1 - t), :], peer.at[s], ts.at[s], tr.at[s], {"tp": 1 - t})

    def along(s, d):
        block = slots.at[s, :, quarter(t, d), :]
        return remote(block, slots.at[s + 1, :, quarter(t, d), :], ags.at[d, s], agr.at[d, s], {"fs": ahead[d]})

    def arrived(s, d):
        block = slots.at[s, :, quarter(t, d), :]
        return remote(block, block, ags.at[d, s - 1], agr.at[d, s - 1], {"fs": ahead[d]})

    def across(s, d, core):
        block = slots.at[s, :, quarter(core, d), :]
        return remote(block, block, aps.at[d, s - 1], apr.at[d, s - 1], {"tp": 1 - t})

    def ring_step(s, carry):
        for d in range(2):
            arrived(s, d).wait_recv()

            @pl.when(s < n - 1)
            def _():
                along(s, d).start()

            across(s, d, t).start()

        @pl.when(s > 1)
        def _():
            for d in range(2):
                across(s - 1, d, 1 - t).wait_recv()

        compute(s - 1)
        trade(s - 1).start()
        return carry

    lax.fori_loop(1, n, ring_step, 0)

    def own(s, o, d):
        return (
            part[s, o, quarter(t, d), :].astype(f32)
            + peer[s, o, d * q:(d + 1) * q, :].astype(f32)
        )

    def trade_done(s):
        remote(peer.at[s], peer.at[s], ts.at[s], tr.at[s], {"tp": 1 - t}).wait_recv()

    def sum_step(s):
        trade_done(s + 1)
        for o in range(2):
            for d in range(2):
                value = own(s + 1, o, d)
                if s > 0:
                    slot = ring_in.at[d, s - 1, o]
                    remote(slot, slot, rs.at[d, s - 1, o], rr.at[d, s - 1, o], {"fs": ahead[d]}).wait_recv()
                    value = value + ring_in[d, s - 1, o].astype(f32)
                ring_out[d, s, o] = value.astype(bf16)
                go(remote(ring_out.at[d, s, o], ring_in.at[d, s, o], rs.at[d, s, o], rr.at[d, s, o], {"fs": ahead[d]}))

    sum_step(0)
    for d in range(2):
        across(n - 1, d, 1 - t).wait_recv()
    compute(n - 1)
    trade(n - 1).start()
    grads[...] = acc[...].astype(bf16)
    order = list(range(1, n)) + [0]
    for k in order:
        g = lax.rem(f + k, n)
        go(remote(grads.at[:, :, span(g * dl + (1 - r) * hl, hl, hl)], x_in.at[k], xs.at[k], xr.at[k], {"rep": 1 - r}))

    def g_block(origin, side):
        return g_out.at[:, span(origin * hid, hid, hid), span(side * hl, hl, hl)]

    def pair_sum(k):
        g = lax.rem(f + k, n)
        remote(x_in.at[k], x_in.at[k], xs.at[k], xr.at[k], {"rep": 1 - r}).wait_recv()
        return (x_in[k].astype(f32) + acc[:, :, span(g * dl + r * hl, hl, hl)]).astype(bf16)

    def pass_on(k):
        origin = lax.rem(f - k + n, n)
        block = g_block(origin, r)
        remote(block, block, gs.at[k - 1], gr.at[k - 1], {"fs": origin}).wait_recv()
        go(remote(block, block, fs_.at[k], fr.at[k], {"rep": 1 - r}))

    for s in range(n - 1):
        if s > 0:
            sum_step(s)
        x_out[s] = pair_sum(s + 1)
        go(remote(x_out.at[s], g_block(f, r), gs.at[s], gr.at[s], {"fs": lax.rem(f + s + 1, n)}))
        if s >= 2:
            pass_on(s - 1)
    g_out[:, span(f * hid, hid, hid), span(r * hl, hl, hl)] = pair_sum(0)
    block = g_block(f, r)
    go(remote(block, block, fs_.at[0], fr.at[0], {"rep": 1 - r}))
    trade_done(0)
    for o in range(2):
        for d in range(2):
            slot = ring_in.at[d, n - 2, o]
            remote(slot, slot, rs.at[d, n - 2, o], rr.at[d, n - 2, o], {"fs": ahead[d]}).wait_recv()
            value = own(0, o, d) + ring_in[d, n - 2, o].astype(f32)
            outs[o][quarter(t, d), :] = value.astype(bf16)
        mine = outs[o].at[half(t), :]
        go(remote(mine, mine, os_.at[o], or_.at[o], {"tp": 1 - t}))
    for k in range(n - 2, n):
        pass_on(k)
    for o in range(2):
        other = outs[o].at[half(1 - t), :]
        remote(other, other, os_.at[o], or_.at[o], {"tp": 1 - t}).wait_recv()
    for k in range(n):
        block = g_block(lax.rem(f - k + n, n), 1 - r)
        remote(block, block, fs_.at[k], fr.at[k], {"rep": 1 - r}).wait_recv()
    for s in range(n):
        trade(s).wait_send()
    for s in range(1, n):
        for d in range(2):
            if s < n - 1:
                along(s, d).wait_send()
            across(s, d, t).wait_send()
    for copy in pending:
        copy.wait_send()


def add_kernel(total, first, second, third, first_new, second_new, third_new):
    for i, (old, new) in enumerate(((first, first_new), (second, second_new), (third, third_new))):
        new[...] = old[...] + total[i].astype(jnp.float32).T


def add_turned(total, sums):
    _, ff, dl = total.shape
    width = 256
    block = pl.BlockSpec((dl, width), lambda i: (0, i))
    return pl.pallas_call(
        add_kernel,
        grid=(ff // width,),
        out_shape=tuple(jax.ShapeDtypeStruct(old.shape, old.dtype) for old in sums),
        in_specs=[pl.BlockSpec((3, width, dl), lambda i: (0, i, 0))] + [block] * 3,
        out_specs=(block,) * 3,
        name="add_turned",
    )(total, *sums)


VMEM = pl.BlockSpec(memory_space=pltpu.VMEM)


def dma(*shape):
    return pltpu.SemaphoreType.DMA(shape)


def split_hidden(
    n,
    later_input,
    earlier_input,
    cotangent,
    gate_weight,
    up_weight,
    down_weight,
    gate_sum,
    up_sum,
    down_sum,
):
    bf16 = jnp.bfloat16
    m, width = later_input.shape
    dl, ff = gate_weight.shape
    hid = ff // n
    hl, q = dl // 2, m // 4
    tokens = jnp.stack([later_input, earlier_input, cotangent])
    weights = jnp.stack([gate_weight.T, up_weight.T, down_weight.T])
    later_output, earlier_input_grad, total = pl.pallas_call(
        functools.partial(fused_kernel, n),
        out_shape=(
            jax.ShapeDtypeStruct((m, width), bf16),
            jax.ShapeDtypeStruct((m, width), bf16),
            jax.ShapeDtypeStruct((3, ff, dl), bf16),
        ),
        in_specs=[VMEM] * 2,
        out_specs=(VMEM, VMEM, VMEM),
        scratch_shapes=[
            pltpu.VMEM((n, 3, m, width), bf16),
            pltpu.VMEM((3, hid, width), bf16),
            pltpu.VMEM((n, 2, m, width), bf16),
            pltpu.VMEM((n, 2, 2 * q, width), bf16),
            pltpu.VMEM((3, hid, width), jnp.float32),
            pltpu.VMEM((3, hid, width), bf16),
            pltpu.VMEM((2, n - 1, 2, q, width), bf16),
            pltpu.VMEM((2, n - 1, 2, q, width), bf16),
            pltpu.VMEM((n, 3, hid, hl), bf16),
            pltpu.VMEM((n - 1, 3, hid, hl), bf16),
        ]
        + [dma(2, n - 1)] * 4
        + [dma(n - 1)] * 4
        + [
            dma(n), dma(n),
            dma(2, n - 1, 2), dma(2, n - 1, 2),
            dma(2), dma(2),
            dma(n), dma(n),
            dma(n - 1), dma(n - 1),
            dma(n), dma(n),
        ],
        compiler_params=pltpu.CompilerParams(
            collective_id=0, has_side_effects=True, vmem_limit_bytes=67043328
        ),
        name="fused",
    )(tokens, weights)
    return (later_output, earlier_input_grad) + tuple(add_turned(total, (gate_sum, up_sum, down_sum)))


def early_parts(gate_early, up_early, hidden_grad):
    sigmoid_gate = jax.nn.sigmoid(gate_early)
    silu_early = gate_early * sigmoid_gate
    gate_grad = (
        hidden_grad * up_early * sigmoid_gate * (1.0 + gate_early * (1.0 - sigmoid_gate))
    ).astype(jnp.bfloat16)
    up_grad = (hidden_grad * silu_early).astype(jnp.bfloat16)
    hidden_early = (silu_early * up_early).astype(jnp.bfloat16)
    return gate_grad, up_grad, hidden_early


def contract_last(first, second):
    return lax.dot_general(
        first, second, (((1,), (1,)), ((), ())), preferred_element_type=jnp.float32
    )


def contract_first(first, second):
    return lax.dot_general(
        first, second, (((0,), (0,)), ((), ())), preferred_element_type=jnp.float32
    )


def per_device(
    later_input,
    earlier_input,
    cotangent,
    gate_weight,
    up_weight,
    down_weight,
    gate_sum,
    up_sum,
    down_sum,
):
    gate_full, up_full, down_full = (
        lax.all_gather(gate_weight, "fs", axis=0, tiled=True),
        lax.all_gather(up_weight, "fs", axis=0, tiled=True),
        lax.all_gather(down_weight, "fs", axis=0, tiled=True),
    )
    gate_late = jnp.dot(later_input, gate_full, preferred_element_type=jnp.float32)
    up_late = jnp.dot(later_input, up_full, preferred_element_type=jnp.float32)
    hidden_late = (jax.nn.silu(gate_late) * up_late).astype(jnp.bfloat16)
    partial_late = contract_last(hidden_late, down_full)
    later_output = lax.psum(partial_late.astype(jnp.bfloat16), "tp")
    gate_early = jnp.dot(earlier_input, gate_full, preferred_element_type=jnp.float32)
    up_early = jnp.dot(earlier_input, up_full, preferred_element_type=jnp.float32)
    hidden_grad = jnp.dot(cotangent, down_full, preferred_element_type=jnp.float32)
    sigmoid_gate = jax.nn.sigmoid(gate_early)
    silu_early = gate_early * sigmoid_gate
    gate_grad = (
        hidden_grad * up_early * sigmoid_gate * (1.0 + gate_early * (1.0 - sigmoid_gate))
    ).astype(jnp.bfloat16)
    up_grad = (hidden_grad * silu_early).astype(jnp.bfloat16)
    hidden_early = (silu_early * up_early).astype(jnp.bfloat16)
    partial_early = contract_last(gate_grad, gate_full) + contract_last(up_grad, up_full)
    earlier_input_grad = lax.psum(partial_early.astype(jnp.bfloat16), "tp")
    columns, cot_columns = (
        lax.all_to_all(earlier_input, "fs", split_axis=1, concat_axis=0, tiled=True),
        lax.all_to_all(cotangent, "fs", split_axis=1, concat_axis=0, tiled=True),
    )
    gate_local = contract_first(columns, lax.all_gather(gate_grad, "fs", axis=0, tiled=True))
    up_local = contract_first(columns, lax.all_gather(up_grad, "fs", axis=0, tiled=True))
    down_local = contract_first(cot_columns, lax.all_gather(hidden_early, "fs", axis=0, tiled=True))
    gate_total, up_total, down_total = (
        lax.psum(gate_local.astype(jnp.bfloat16), "rep").astype(jnp.float32),
        lax.psum(up_local.astype(jnp.bfloat16), "rep").astype(jnp.float32),
        lax.psum(down_local.astype(jnp.bfloat16), "rep").astype(jnp.float32),
    )
    return (
        later_output,
        earlier_input_grad,
        gate_sum + gate_total,
        up_sum + up_total,
        down_sum + down_total,
    )


def solution(mesh):
    placed = (
        P(("rep", "fs"), None),
        P(("rep", "fs"), None),
        P(("rep", "fs"), None),
        P("fs", "tp"),
        P("fs", "tp"),
        P("fs", "tp"),
        P("fs", "tp"),
        P("fs", "tp"),
        P("fs", "tp"),
    )
    reps, shards, blocks = (mesh.shape[axis] for axis in ("rep", "fs", "tp"))

    def chosen(*arrays):
        rows = arrays[0].shape[0]
        depth, units = arrays[3].shape
        fits = (
            reps == 2
            and blocks == 2
            and shards % 2 == 0
            and units % (shards * 16) == 0
            and depth % 256 == 0
            and rows % 64 == 0
            and units % 256 == 0
            and arrays[0].shape[1] % 512 == 0
        )
        return split_hidden(shards, *arrays) if fits else per_device(*arrays)

    return jax.shard_map(
        chosen,
        mesh=mesh,
        in_specs=placed,
        out_specs=(
            P(("rep", "fs"), None),
            P(("rep", "fs"), None),
            P("fs", "tp"),
            P("fs", "tp"),
            P("fs", "tp"),
        ),
        check_vma=False,
    )
```

time: 246 us -> 202 us (0.82)
  matrix products: 22.2 us -> 0 us
  local copies, waits for them, and re-layouts: 24.5 us -> 3.73 us
  other arithmetic: 9.41 us -> 2.99 us
  Pallas kernels: 189 us -> 194 us
    dot_general x9 -> x0, matrix products: 22.2 us -> none  [the longest x3 11.1 us: contract_last(): lax.dot_general(first, second, (((1,), (1,)), ((), ())), preferred_elemen...]
    unnamed x39 -> x19, local copies, waits for them, and re-layouts: 16.1 us -> 3.73 us
    slice x1 -> x0, local copies, waits for them, and re-layouts: 8.39 us -> none  [split_hidden(): both = tok[:2].reshape(2 * count, width)]
    pallas_call x2, Pallas kernels: 189 us -> 194 us  [the longest x1 188 us: split_hidden(): pl.pallas_call(functools.partial(fused_kernel, n), out_shape=(jax.ShapeDt...]
    add x1 -> x0, other arithmetic: 4.69 us -> none  [split_hidden(): down_sum + total[2].T.astype(jnp.float32)]
where the time goes in v2:
time: 202 us
  Pallas kernels  194 us (96%)
  local copies, waits for them, and re-layouts  3.73 us (2%)
  other arithmetic  2.99 us (1%)
    pallas_call x1, Pallas kernels, split_hidden(): pl.pallas_call(functools.partial(fused_kernel, n), out_shape=(jax.ShapeDt...  188 us
    pallas_call x1, Pallas kernels, add_turned(): pl.pallas_call(add_kernel, grid=(ff // width,), out_shape=tuple((jax.Shap...  6.6 us

profile of v2, /device:TPU:16, one launch (start us, length us, event | category | flops | bytes accessed | tf_op | source)
XLA Modules:
  0.0 201.7 jit_solution(10325025494281970889)
XLA Ops:
  0.6 0.0 copy-start
  0.6 0.0 copy-start.1
  0.7 1.5 copy.14
  2.2 0.0 copy-done
  2.2 0.3 copy.15
  2.5 0.0 copy-done.1
  2.5 0.3 copy.16
  2.7 0.0 copy-start.4
  2.8 0.0 copy-start.5
  2.8 0.0 copy-start.6
  2.8 1.7 pad_maximum_fusion.wt
  4.5 0.0 copy-done.4
  4.5 0.0 copy-done.5
  4.5 0.1 copy-done.6
  4.5 1.3 pad_maximum_fusion.1.tok
  5.8 187.7 %fused.1 = (bf16[128,2048]{1,0:T(8,128)(2,1)}, bf16[128,2048]{1,0:T(8,128)(2,1)}, bf16[3,1536,256]{2,1,0:T(8,128)(2,1)}) custom-call(bf16[3,128,2048]{2,1,0:T(8,128)(2,1)} %pad_maximum_fusion.1.tok, bf16[3,1536,256]{2,1,0:T(8,128)(2,1)} %pad_maximum_fusion.wt), custom_call_target="tpu_custom_call" | custom-call | tf_op jit(solution)/shard_map/fused/pallas_call | solution.py:286
  193.5 0.0 copy-start.3
  193.5 0.0 copy-start.2
  193.5 6.6 %add_turned.1 = (f32[256,1536]{1,0:T(8,128)}, f32[256,1536]{1,0:T(8,128)}, f32[256,1536]{1,0:T(8,128)}) custom-call(bf16[3,1536,256]{2,1,0:T(8,128)(2,1)} %get-tuple-element.13.total, f32[256,1536]{1,0:T(8,128)} %first.1, f32[256,1536]{1,0:T(8,128)} %second.1, f32[256,1536]{1,0:T(8,128)} %third.1), custom_call_target="tpu_custom_call" | custom-call | tf_op jit(solution)/shard_map/add_turned/pallas_call | solution.py:250
  200.1 0.0 copy-done.3
  200.1 0.8 copy.19
  200.9 0.0 copy-done.2
  200.9 0.8 copy.20
Async XLA Ops:
  0.6 1.5 copy-start
  0.6 1.8 copy-start.1
  2.7 1.7 copy-start.4
  2.8 1.7 copy-start.5
  2.8 1.7 copy-start.6
  193.5 6.6 %copy-start.3 = (bf16[128,2048]{1,0:T(8,128)(2,1)S(1)}, bf16[128,2048]{1,0:T(8,128)(2,1)}, u32[]{:S(2)}) copy-start(bf16[128,2048]{1,0:T(8,128)(2,1)} %get-tuple-element.22) | copy-start | bytes 1572868
  193.5 7.4 %copy-start.2 = (bf16[128,2048]{1,0:T(8,128)(2,1)S(1)}, bf16[128,2048]{1,0:T(8,128)(2,1)}, u32[]{:S(2)}) copy-start(bf16[128,2048]{1,0:T(8,128)(2,1)} %get-tuple-element.23) | copy-start | bytes 1572868

commit v3 on v2

--- a/solution.py
+++ b/solution.py
@@ -78,6 +78,28 @@
     def piece(origin, side):
         return w.at[:, :, span(origin * dl + side * hl, hl, hl)]
 
+    def along(s, d):
+        block = slots.at[s, :, quarter(t, d), :]
+        return remote(block, slots.at[s + 1, :, quarter(t, d), :], ags.at[d, s], agr.at[d, s], {"fs": ahead[d]})
+
+    def arrived(s, d):
+        block = slots.at[s, :, quarter(t, d), :]
+        return remote(block, block, ags.at[d, s - 1], agr.at[d, s - 1], {"fs": ahead[d]})
+
+    def across(s, d, core):
+        block = slots.at[s, :, quarter(core, d), :]
+        return remote(block, block, aps.at[d, s - 1], apr.at[d, s - 1], {"tp": 1 - t})
+
+    def take_on(s):
+        for d in range(2):
+            arrived(s, d).wait_recv()
+
+            @pl.when(s < n - 1)
+            def _():
+                along(s, d).start()
+
+            across(s, d, t).start()
+
     for k in range(1, n):
         g = lax.rem(f + k, n)
         go(remote(
@@ -94,6 +116,7 @@
         block = piece(origin, r)
         remote(block, block, ws.at[k - 1], wr.at[k - 1], {"fs": origin}).wait_recv()
         go(remote(block, block, wxs.at[k - 1], wxr.at[k - 1], {"rep": 1 - r}))
+    take_on(1)
     for k in range(1, n):
         block = piece(lax.rem(f - k + n, n), 1 - r)
         remote(block, block, wxs.at[k - 1], wxr.at[k - 1], {"rep": 1 - r}).wait_recv()
@@ -121,27 +144,10 @@
     def trade(s):
         return remote(part.at[s, :, half(1 - t), :], peer.at[s], ts.at[s], tr.at[s], {"tp": 1 - t})
 
-    def along(s, d):
-        block = slots.at[s, :, quarter(t, d), :]
-        return remote(block, slots.at[s + 1, :, quarter(t, d), :], ags.at[d, s], agr.at[d, s], {"fs": ahead[d]})
-
-    def arrived(s, d):
-        block = slots.at[s, :, quarter(t, d), :]
-        return remote(block, block, ags.at[d, s - 1], agr.at[d, s - 1], {"fs": ahead[d]})
-
-    def across(s, d, core):
-        block = slots.at[s, :, quarter(core, d), :]
-        return remote(block, block, aps.at[d, s - 1], apr.at[d, s - 1], {"tp": 1 - t})
-
     def ring_step(s, carry):
-        for d in range(2):
-            arrived(s, d).wait_recv()
-
-            @pl.when(s < n - 1)
-            def _():
-                along(s, d).start()
-
-            across(s, d, t).start()
+        @pl.when(s > 1)
+        def _():
+            take_on(s)
 
         @pl.when(s > 1)
         def _():
@@ -205,8 +211,8 @@
             sum_step(s)
         x_out[s] = pair_sum(s + 1)
         go(remote(x_out.at[s], g_block(f, r), gs.at[s], gr.at[s], {"fs": lax.rem(f + s + 1, n)}))
-        if s >= 2:
-            pass_on(s - 1)
+        if s >= 1:
+            pass_on(s)
     g_out[:, span(f * hid, hid, hid), span(r * hl, hl, hl)] = pair_sum(0)
     block = g_block(f, r)
     go(remote(block, block, fs_.at[0], fr.at[0], {"rep": 1 - r}))
@@ -219,7 +225,7 @@
             outs[o][quarter(t, d), :] = value.astype(bf16)
         mine = outs[o].at[half(t), :]
         go(remote(mine, mine, os_.at[o], or_.at[o], {"tp": 1 - t}))
-    for k in range(n - 2, n):
+    for k in range(n - 1, n):
         pass_on(k)
     for o in range(2):
         other = outs[o].at[half(1 - t), :]

time: 202 us -> 187 us (0.926)
  Pallas kernels: 194 us -> 178 us
    pallas_call x1, Pallas kernels: 188 us -> 172 us  [split_hidden(): pl.pallas_call(functools.partial(fused_kernel, n), out_shape=(jax.ShapeDt...]
where the time goes in v3:
time: 187 us; the launch traced here: 186 us
  Pallas kernels  178 us (95%)
  local copies, waits for them, and re-layouts  3.73 us (2%)
  other arithmetic  2.99 us (2%)
    pallas_call x1, Pallas kernels, split_hidden(): pl.pallas_call(functools.partial(fused_kernel, n), out_shape=(jax.ShapeDt...  172 us
    pallas_call x1, Pallas kernels, add_turned(): pl.pallas_call(add_kernel, grid=(ff // width,), out_shape=tuple((jax.Shap...  6.6 us

profile of v3, /device:TPU:16, one launch (start us, length us, event | category | flops | bytes accessed | tf_op | source)
XLA Modules:
  0.0 185.9 jit_solution(2397838190572277713)
XLA Ops:
  0.6 0.0 copy-start
  0.6 0.0 copy-start.1
  0.7 1.5 copy.14
  2.2 0.0 copy-done
  2.2 0.3 copy.15
  2.5 0.0 copy-done.1
  2.5 0.3 copy.16
  2.7 0.0 copy-start.4
  2.8 0.0 copy-start.5
  2.8 0.0 copy-start.6
  2.8 1.7 pad_maximum_fusion.wt
  4.5 0.0 copy-done.4
  4.5 0.0 copy-done.5
  4.5 0.1 copy-done.6
  4.5 1.3 pad_maximum_fusion.1.tok
  5.8 171.9 %fused.1 = (bf16[128,2048]{1,0:T(8,128)(2,1)}, bf16[128,2048]{1,0:T(8,128)(2,1)}, bf16[3,1536,256]{2,1,0:T(8,128)(2,1)}) custom-call(bf16[3,128,2048]{2,1,0:T(8,128)(2,1)} %pad_maximum_fusion.1.tok, bf16[3,1536,256]{2,1,0:T(8,128)(2,1)} %pad_maximum_fusion.wt), custom_call_target="tpu_custom_call" | custom-call | tf_op jit(solution)/shard_map/fused/pallas_call | solution.py:292
  177.7 0.0 copy-start.3
  177.7 0.0 copy-start.2
  177.7 6.6 %add_turned.1 = (f32[256,1536]{1,0:T(8,128)}, f32[256,1536]{1,0:T(8,128)}, f32[256,1536]{1,0:T(8,128)}) custom-call(bf16[3,1536,256]{2,1,0:T(8,128)(2,1)} %get-tuple-element.13.total, f32[256,1536]{1,0:T(8,128)} %first.1, f32[256,1536]{1,0:T(8,128)} %second.1, f32[256,1536]{1,0:T(8,128)} %third.1), custom_call_target="tpu_custom_call" | custom-call | tf_op jit(solution)/shard_map/add_turned/pallas_call | solution.py:256
  184.3 0.0 copy-done.3
  184.3 0.8 copy.19
  185.1 0.0 copy-done.2
  185.1 0.8 copy.20
Async XLA Ops:
  0.6 1.5 copy-start
  0.6 1.8 copy-start.1
  2.7 1.7 copy-start.4
  2.8 1.7 copy-start.5
  2.8 1.7 copy-start.6
  177.7 6.6 %copy-start.3 = (bf16[128,2048]{1,0:T(8,128)(2,1)S(1)}, bf16[128,2048]{1,0:T(8,128)(2,1)}, u32[]{:S(2)}) copy-start(bf16[128,2048]{1,0:T(8,128)(2,1)} %get-tuple-element.22) | copy-start | bytes 1572868
  177.7 7.4 %copy-start.2 = (bf16[128,2048]{1,0:T(8,128)(2,1)S(1)}, bf16[128,2048]{1,0:T(8,128)(2,1)}, u32[]{:S(2)}) copy-start(bf16[128,2048]{1,0:T(8,128)(2,1)} %get-tuple-element.23) | copy-start | bytes 1572868
